TPU v7x, 32 devices: a whole 2x2x4 slice. The times are simulated.
32 devices in a mesh: fs: 8 (over z, y), tp: 4 (over x, core).
Axes of the slice: x: 2, y: 2, z: 4, core: 2. Of those that a mesh axis runs over, the one named last changes fastest.
Arguments:
- layer_input: bfloat16 [20480, 4096], P('fs'), may hold values from -140 to 140
- query_cotangent: bfloat16 [20480, 2048], P('fs', 'tp'), may hold values from -0.46817673 to 0.46817673
- value_cotangent: bfloat16 [20480, 512], P('fs', 'tp'), may hold values from -0.46817673 to 0.46817673
- query_weight: float32 [4096, 2048], P('fs', 'tp'), may hold values from -0.09375 to 0.09375
- value_weight: float32 [4096, 512], P('fs', 'tp'), may hold values from -0.09375 to 0.09375
- query_moment: float32 [4096, 2048], P('fs', 'tp'), may hold values from -18 to 18
- value_moment: float32 [4096, 512], P('fs', 'tp'), may hold values from -18 to 18
- query_left_stat: float32 [16, 256, 256], P('fs'), may hold values from -24 to 24
- value_left_stat: float32 [16, 256, 256], P('fs'), may hold values from -24 to 24
- query_right_stat: float32 [32, 64, 64], P('tp'), may hold values from -24 to 24
- value_right_stat: float32 [8, 64, 64], P('tp'), may hold values from -24 to 24
- query_left_root: bfloat16 [16, 256, 256], P('fs'), may hold values from -1.5 to 2
- value_left_root: bfloat16 [16, 256, 256], P('fs'), may hold values from -1.5 to 2
- query_right_root: bfloat16 [32, 64, 64], P('tp'), may hold values from -1.5 to 2
- value_right_root: bfloat16 [8, 64, 64], P('tp'), may hold values from -1.5 to 2
Outputs:
- query_update: float32 [4096, 2048], P('fs', 'tp')
- value_update: float32 [4096, 512], P('fs', 'tp')
- query_moment_new: float32 [4096, 2048], P('fs', 'tp')
- value_moment_new: float32 [4096, 512], P('fs', 'tp')
- query_left_new: float32 [16, 256, 256], P('fs')
- value_left_new: float32 [16, 256, 256], P('fs')
- query_right_new: float32 [32, 64, 64], P('tp')
- value_right_new: float32 [8, 64, 64], P('tp')
- query_copy: bfloat16 [4096, 2048], P(None, 'tp')
- value_copy: bfloat16 [4096, 512], P(None, 'tp')
All inputs are finite; a program needn't handle non-finite values.
Results may differ from a plain program's by a relative error of at most 0.0075.
Values may be sent and summed in bfloat16 or wider, within the bound.
A program may use at most 128 MiB of HBM per device.

v0:
```python
import jax
import jax.numpy as jnp
from jax import lax
from jax.sharding import PartitionSpec as P

D = 4096
HEAD = 64
BLOCK = 256
Q_COLS = 2048
V_COLS = 512
momentum_decay = 0.9
statistic_decay = 0.9
learning_rate = 0.002
epsilon = 1e-06
highest = lax.Precision.HIGHEST


def token_sum(inputs, cotangent):
    return lax.dot_general(
        inputs, cotangent, (((0,), (0,)), ((), ())), preferred_element_type=jnp.float32
    )


def precondition(moment, left_root, right_root):
    shard_rows, columns = moment.shape
    head_count = columns // HEAD
    by_head = jnp.einsum(
        "rhk,hkl->rhl",
        moment.reshape(shard_rows, head_count, HEAD),
        right_root.astype(jnp.float32),
        precision=highest,
    )
    by_block = by_head.reshape(shard_rows // BLOCK, BLOCK, columns)
    return jnp.einsum(
        "bij,bjc->bic", left_root.astype(jnp.float32), by_block, precision=highest
    ).reshape(shard_rows, columns)


def local_terms(gradient, moment, left_root, right_root):
    shard_rows, columns = gradient.shape
    moment_new = momentum_decay * moment + (1.0 - momentum_decay) * gradient
    blocks = gradient.reshape(shard_rows // BLOCK, BLOCK, columns)
    left_part = jnp.einsum("bic,bjc->bij", blocks, blocks, precision=highest)
    per_head = gradient.reshape(shard_rows, columns // HEAD, HEAD)
    right_part = jnp.einsum("rhk,rhl->hkl", per_head, per_head, precision=highest)
    direction = precondition(moment_new, left_root, right_root)
    squares = jnp.stack([jnp.sum(moment_new * moment_new), jnp.sum(direction * direction)])
    return (moment_new, left_part, right_part, direction, squares)


def local(
    layer_input,
    query_cotangent,
    value_cotangent,
    query_weight,
    value_weight,
    query_moment,
    value_moment,
    query_left_stat,
    value_left_stat,
    query_right_stat,
    value_right_stat,
    query_left_root,
    value_left_root,
    query_right_root,
    value_right_root,
):
    query_width = query_cotangent.shape[1]
    both_cotangents = jnp.concatenate([query_cotangent, value_cotangent], axis=1)
    both_gradients = lax.psum_scatter(
        token_sum(layer_input, both_cotangents), "fs", scatter_dimension=0, tiled=True
    )
    query_gradient = both_gradients[:, :query_width]
    value_gradient = both_gradients[:, query_width:]
    query_moment_new, query_left_part, query_right_part, query_direction, query_squares = (
        local_terms(query_gradient, query_moment, query_left_root, query_right_root)
    )
    value_moment_new, value_left_part, value_right_part, value_direction, value_squares = (
        local_terms(value_gradient, value_moment, value_left_root, value_right_root)
    )
    squares = jnp.concatenate([query_squares, value_squares])
    query_right_sum, value_right_sum = (
        lax.psum(query_right_part.astype(jnp.bfloat16), "fs").astype(jnp.float32),
        lax.psum(value_right_part.astype(jnp.bfloat16), "fs").astype(jnp.float32),
    )
    query_left_sum, value_left_sum = (
        lax.psum(query_left_part.astype(jnp.bfloat16), "tp").astype(jnp.float32),
        lax.psum(value_left_part.astype(jnp.bfloat16), "tp").astype(jnp.float32),
    )
    all_squares = lax.psum(squares, ("fs", "tp"))
    query_left_new = (
        statistic_decay * query_left_stat + (1.0 - statistic_decay) / Q_COLS * query_left_sum
    )
    value_left_new = (
        statistic_decay * value_left_stat + (1.0 - statistic_decay) / V_COLS * value_left_sum
    )
    query_right_new = (
        statistic_decay * query_right_stat + (1.0 - statistic_decay) / D * query_right_sum
    )
    value_right_new = (
        statistic_decay * value_right_stat + (1.0 - statistic_decay) / D * value_right_sum
    )
    query_update = jnp.sqrt(all_squares[0] / (all_squares[1] + epsilon)) * query_direction
    value_update = jnp.sqrt(all_squares[2] / (all_squares[3] + epsilon)) * value_direction
    query_shard = (query_weight - learning_rate * query_update).astype(jnp.bfloat16)
    value_shard = (value_weight - learning_rate * value_update).astype(jnp.bfloat16)
    query_copy, value_copy = (
        lax.all_gather(query_shard, "fs", axis=0, tiled=True),
        lax.all_gather(value_shard, "fs", axis=0, tiled=True),
    )
    return (
        query_update,
        value_update,
        query_moment_new,
        value_moment_new,
        query_left_new,
        value_left_new,
        query_right_new,
        value_right_new,
        query_copy,
        value_copy,
    )


def solution(mesh):
    placed = (
        P("fs", None),
        P("fs", "tp"),
        P("fs", "tp"),
        P("fs", "tp"),
        P("fs", "tp"),
        P("fs", "tp"),
        P("fs", "tp"),
        P("fs", None, None),
        P("fs", None, None),
        P("tp", None, None),
        P("tp", None, None),
        P("fs", None, None),
        P("fs", None, None),
        P("tp", None, None),
        P("tp", None, None),
    )
    return jax.shard_map(
        local,
        mesh=mesh,
        in_specs=placed,
        out_specs=(
            P("fs", "tp"),
            P("fs", "tp"),
            P("fs", "tp"),
            P("fs", "tp"),
            P("fs", None, None),
            P("fs", None, None),
            P("tp", None, None),
            P("tp", None, None),
            P(None, "tp"),
            P(None, "tp"),
        ),
        check_vma=False,
    )
```

profile of v0, /device:TPU:0, one launch (start us, length us, event | category | flops | bytes accessed | tf_op | source)
XLA Modules:
  0.0 512.9 jit_solution(3195955658530197964)
XLA Ops:
  7.2 21.4 %convolution_bitcast_fusion = f32[4096,640]{0,1:T(8,128)} fusion(bf16[2560,4096]{1,0:T(8,128)(2,1)} %param.15, bf16[2560,128]{1,0:T(8,128)(2,1)} %param.17, bf16[2560,512]{1,0:T(8,128)(2,1)} %param.16), kind=kOutput, calls=%fused_computation | convolution fusion | flops 13428326400 | bytes 34734080 | tf_op jit(solution)/shard_map/dot_general | solution.py:19
  28.7 1.1 copy-done.4
  31.0 179.1 %reduce-scatter.2.cloned.1.call-done = f32[512,640]{0,1:T(8,128)} async-done(((f32[4096,640]{0,1:T(8,128)}), f32[512,640]{0,1:T(8,128)}) %reduce-scatter.2.cloned.1.call-update) | async-done | bytes 1310736 | tf_op jit(solution)/shard_map/reduce_scatter | solution.py:70
  210.1 2.2 multiply_reduce_fusion.1
  212.3 1.6 convolution_bitcast_fusion.1
  213.9 1.9 reshape.59
  215.8 2.4 multiply_reduce_fusion.3
  218.9 1.8 convolution_bitcast_fusion.2
  220.7 1.8 reshape.61
  222.5 2.3 multiply_reduce_fusion
  224.8 2.7 multiply_reduce_fusion.2
  227.5 2.7 pad_maximum_fusion
  230.2 39.4 %psum.35 = f32[4]{0:T(128)S(1)} all-reduce(f32[4]{0:T(128)S(1)} %pad_maximum_fusion), channel_id=1, replica_groups=mesh['fs'=8,'tp'=4] {'fs','tp'}, use_global_device_ids=true, to_apply=%region_5.0 | all-reduce | flops 4 | bytes 32 | tf_op jit(solution)/shard_map/psum | solution.py:90
  270.0 1.9 convolution_convert_fusion
  271.8 1.9 copy.53
  273.7 2.3 convolution_convert_fusion.1
  276.0 1.7 convolution_convert_fusion.2
  279.8 1.0 multiply_bitcast_fusion
  280.9 1.7 subtract_convert_fusion.1
  284.3 2.6 subtract_convert_fusion
  286.8 1.3 copy.48
  288.2 1.8 copy.49
  289.9 1.5 convolution_convert_fusion.3
  291.4 36.9 %psum.39 = bf16[2,64,64]{2,1,0:T(8,128)(2,1)S(1)} all-reduce(bf16[2,64,64]{2,1,0:T(8,128)(2,1)S(1)} %convolution_convert_fusion.3), channel_id=1, replica_groups=mesh['fs'=8,'tp'=4] {'fs'}, use_global_device_ids=true, to_apply=%region_9.0 | all-reduce | flops 8192 | bytes 32768 | tf_op jit(solution)/shard_map/psum | solution.py:84
  329.0 19.2 %all-reduce.4.cloned.1.call-done = bf16[8,64,64]{2,1,0:T(8,128)(2,1)} async-done(((bf16[8,64,64]{2,1,0:T(8,128)(2,1)}), bf16[8,64,64]{2,1,0:T(8,128)(2,1)}) %all-reduce.4.cloned.1.call-update) | async-done | bytes 65552 | tf_op jit(solution)/shard_map/psum | solution.py:83
  348.1 1.8 multiply_add_fusion.3
  349.9 34.4 %all-reduce.6.cloned.1.call-done = (bf16[2,256,256]{2,1,0:T(8,128)(2,1)}, bf16[2,256,256]{2,1,0:T(8,128)(2,1)}) async-done(((bf16[2,256,256]{2,1,0:T(8,128)(2,1)}, bf16[2,256,256]{2,1,0:T(8,128)(2,1)}), (bf16[2,256,256]{2,1,0:T(8,128)(2,1)}, bf16[2,256,256]{2,1,0:T(8,128)(2,1)})) %all-reduce.6.cloned.1.call-update) | async-done | bytes 524304 | tf_op jit(solution)/shard_map/psum | solution.py:87
  384.3 2.2 multiply_add_fusion.1
  386.5 40.3 %all-gather.5.cloned.1.call-done = bf16[4096,128]{1,0:T(8,128)(2,1)} async-done(((bf16[512,128]{1,0:T(8,128)(2,1)}), bf16[4096,128]{1,0:T(8,128)(2,1)}) %all-gather.5.cloned.1.call-update) | async-done | bytes 1048592 | tf_op jit(solution)/shard_map/all_gather | solution.py:109
  426.7 74.1 %all-gather.3.cloned.1.call-done = bf16[4096,512]{1,0:T(8,128)(2,1)} async-done(((bf16[512,512]{1,0:T(8,128)(2,1)}), bf16[4096,512]{1,0:T(8,128)(2,1)}) %all-gather.3.cloned.1.call-update) | async-done | bytes 4194320 | tf_op jit(solution)/shard_map/all_gather | solution.py:108
  500.8 4.6 copy.67
  505.4 1.0 copy.68
  (40 shorter events, 4.0 us)
Async XLA Ops:
  7.2 215.3 %copy-start = (bf16[2,256,256]{2,1,0:T(8,128)(2,1)S(1)}, bf16[2,256,256]{2,1,0:T(8,128)(2,1)}, u32[]{:S(2)}) copy-start(bf16[2,256,256]{2,1,0:T(8,128)(2,1)} %param.26) | copy-start | bytes 786436
  7.2 202.9 %reduce-scatter.2.cloned.1.call-start = ((), (), s32[]{:S(2)}) async-start(), calls=%async_computation.1 | async-start | bytes 11796480 | tf_op jit(solution)/shard_map/reduce_scatter | solution.py:70
  28.6 1.2 copy-start.4
  28.6 1.6 copy-start.9
  28.6 183.7 %copy-start.10 = (bf16[8,64,64]{2,1,0:T(8,128)(2,1)S(1)}, bf16[8,64,64]{2,1,0:T(8,128)(2,1)}, u32[]{:S(2)}) copy-start(bf16[8,64,64]{2,1,0:T(8,128)(2,1)} %param.28) | copy-start | bytes 196612
  28.6 319.5 %all-reduce.4.cloned.1.call-start = ((), (), s32[]{:S(2)}) async-start(), calls=%async_computation.2 | async-start | bytes 262144 | tf_op jit(solution)/shard_map/psum | solution.py:83
  218.2 0.7 copy-start.3
  271.8 12.3 %copy-start.1 = (f32[2,512,256]{1,2,0:T(8,128)S(1)}, f32[2,512,256]{1,2,0:T(8,128)}, u32[]{:S(2)}) copy-start(f32[2,512,256]{1,2,0:T(8,128)} %get-tuple-element.45) | copy-start | bytes 3145732
  277.8 106.6 %all-reduce.6.cloned.1.call-start = ((), (), s32[]{:S(2)}) async-start(), calls=%async_computation.5 | async-start | bytes 1048576 | tf_op jit(solution)/shard_map/psum | solution.py:87
  279.8 147.0 %all-gather.5.cloned.1.call-start = ((), (), s32[]{:S(2)}) async-start(), calls=%async_computation.4 | async-start | bytes 1179648 | tf_op jit(solution)/shard_map/all_gather | solution.py:109
  280.9 3.2 copy-start.6
  282.7 218.1 %all-gather.3.cloned.1.call-start = ((), (), s32[]{:S(2)}) async-start(), calls=%async_computation.3 | async-start | bytes 4718592 | tf_op jit(solution)/shard_map/all_gather | solution.py:108
  284.1 44.2 %copy-start.11 = (f32[2,64,64]{2,1,0:T(8,128)S(1)}, f32[2,64,64]{2,1,0:T(8,128)}, u32[]{:S(2)}) copy-start(f32[2,64,64]{2,1,0:T(8,128)} %param.25) | copy-start | bytes 98308
  284.2 102.3 %copy-start.2 = (f32[2,512,256]{1,2,0:T(8,128)}, f32[2,512,256]{1,2,0:T(8,128)S(1)}, u32[]{:S(2)}) copy-start(f32[2,512,256]{1,2,0:T(8,128)S(1)} %broadcast_multiply_fusion) | copy-start | bytes 3145732
  284.2 100.1 %copy-start.7 = (f32[2,256,256]{2,1,0:T(8,128)S(1)}, f32[2,256,256]{2,1,0:T(8,128)}, u32[]{:S(2)}) copy-start(f32[2,256,256]{2,1,0:T(8,128)} %param.23) | copy-start | bytes 1572868
  284.2 100.1 %copy-start.8 = (f32[2,256,256]{2,1,0:T(8,128)S(1)}, f32[2,256,256]{2,1,0:T(8,128)}, u32[]{:S(2)}) copy-start(f32[2,256,256]{2,1,0:T(8,128)} %param.22) | copy-start | bytes 1572868
  500.8 4.6 copy-start.5
Sparse Core Ops, SparseCore 0:
  28.8 181.3 reduce-scatter.1
  277.9 70.1 all-reduce.3
  351.7 32.5 all-reduce.5
  386.3 40.3 all-gather.4
  429.3 71.4 all-gather.2
where the time goes:
time: 514 us; the launch traced here: 513 us
  waiting for transfers between devices  347 us (68%)
  blocking collectives  76.3 us (15%)
  matrix products  37.1 us (7%)
  local copies, waits for them, and re-layouts  18.3 us (4%)
  other arithmetic  17.2 us (3%)
  between operations  16.6 us (3%)
    reduce_scatter x1, waiting for transfers between devices, local(): lax.psum_scatter(token_sum(layer_input, both_cotangents), 'fs', scatter_d...  179 us
    all_gather x1, waiting for transfers between devices, local(): lax.all_gather(query_shard, 'fs', axis=0, tiled=True)  74.1 us
    all_gather x1, waiting for transfers between devices, local(): lax.all_gather(value_shard, 'fs', axis=0, tiled=True)  40.3 us
    psum x1, blocking collectives, local(): all_squares = lax.psum(squares, ('fs', 'tp'))  39.4 us
    psum x1, blocking collectives, local(): lax.psum(value_right_part.astype(jnp.bfloat16), 'fs').astype(jnp.float32)  36.9 us
    psum x1, waiting for transfers between devices, local(): lax.psum(query_left_part.astype(jnp.bfloat16), 'tp').astype(jnp.float32)  34.4 us
    dot_general x1, matrix products, token_sum(): lax.dot_general(inputs, cotangent, (((0,), (0,)), ((), ())), preferred_el...  21.4 us
    psum x1, waiting for transfers between devices, local(): lax.psum(query_right_part.astype(jnp.bfloat16), 'fs').astype(jnp.float32)  19.2 us
  transfers between devices with their start and end apart: 5, of which 5 were waited for; matrix products, arithmetic and copies ran while one was open for 3% of the time, Pallas kernels for 0%

commit v1 on v0

--- a/solution.py
+++ b/solution.py
@@ -87,7 +87,9 @@
         lax.psum(query_left_part.astype(jnp.bfloat16), "tp").astype(jnp.float32),
         lax.psum(value_left_part.astype(jnp.bfloat16), "tp").astype(jnp.float32),
     )
-    all_squares = lax.psum(squares, ("fs", "tp"))
+    all_squares = squares
+    for axis in ("tp", "fs"):
+        all_squares = lax.psum(all_squares, axis)
     query_left_new = (
         statistic_decay * query_left_stat + (1.0 - statistic_decay) / Q_COLS * query_left_sum
     )

time: 514 us -> 497 us (0.967)
  blocking collectives: 76.3 us -> 59.5 us
    psum x1 -> x2, blocking collectives: 39.4 us -> 26.4 us  [local(): all_squares = lax.psum(all_squares, axis)]
where the time goes in v1:
time: 497 us; the launch traced here: 496 us
  waiting for transfers between devices  347 us (70%)
  blocking collectives  59.5 us (12%)
  matrix products  37.1 us (7%)
  local copies, waits for them, and re-layouts  18.3 us (4%)
  other arithmetic  17.2 us (3%)
  between operations  16.6 us (3%)
    reduce_scatter x1, waiting for transfers between devices, local(): lax.psum_scatter(token_sum(layer_input, both_cotangents), 'fs', scatter_d...  179 us
    all_gather x1, waiting for transfers between devices, local(): lax.all_gather(query_shard, 'fs', axis=0, tiled=True)  74.1 us
    all_gather x1, waiting for transfers between devices, local(): lax.all_gather(value_shard, 'fs', axis=0, tiled=True)  40.3 us
    psum x1, waiting for transfers between devices, local(): lax.psum(query_left_part.astype(jnp.bfloat16), 'tp').astype(jnp.float32)  34.4 us
    psum x1, blocking collectives, local(): lax.psum(value_right_part.astype(jnp.bfloat16), 'fs').astype(jnp.float32)  33 us
    psum x2, blocking collectives, local(): all_squares = lax.psum(all_squares, axis)  26.4 us
    dot_general x1, matrix products, token_sum(): lax.dot_general(inputs, cotangent, (((0,), (0,)), ((), ())), preferred_el...  21.3 us
    psum x1, waiting for transfers between devices, local(): lax.psum(query_right_part.astype(jnp.bfloat16), 'fs').astype(jnp.float32)  19.5 us
  transfers between devices with their start and end apart: 5, of which 5 were waited for; matrix products, arithmetic and copies ran while one was open for 3% of the time, Pallas kernels for 0%

profile of v1, /device:TPU:0, one launch (start us, length us, event | category | flops | bytes accessed | tf_op | source)
XLA Modules:
  0.0 496.3 jit_solution(1870781038408484861)
XLA Ops:
  7.2 21.3 %convolution_bitcast_fusion = f32[4096,640]{0,1:T(8,128)} fusion(bf16[2560,4096]{1,0:T(8,128)(2,1)} %param.15, bf16[2560,128]{1,0:T(8,128)(2,1)} %param.17, bf16[2560,512]{1,0:T(8,128)(2,1)} %param.16), kind=kOutput, calls=%fused_computation | convolution fusion | flops 13428326400 | bytes 34734080 | tf_op jit(solution)/shard_map/dot_general | solution.py:19
  28.6 1.1 copy-done.4
  30.9 179.1 %reduce-scatter.2.cloned.1.call-done = f32[512,640]{0,1:T(8,128)} async-done(((f32[4096,640]{0,1:T(8,128)}), f32[512,640]{0,1:T(8,128)}) %reduce-scatter.2.cloned.1.call-update) | async-done | bytes 1310736 | tf_op jit(solution)/shard_map/reduce_scatter | solution.py:70
  210.1 2.2 multiply_reduce_fusion.1
  212.3 1.6 convolution_bitcast_fusion.1
  213.9 1.9 reshape.59
  215.8 2.4 multiply_reduce_fusion.3
  218.8 1.8 convolution_bitcast_fusion.2
  220.6 1.8 reshape.61
  222.4 2.3 multiply_reduce_fusion
  224.7 2.7 multiply_reduce_fusion.2
  227.4 2.7 pad_maximum_fusion
  230.1 6.5 %psum.42 = f32[4]{0:T(128)S(1)} all-reduce(f32[4]{0:T(128)S(1)} %pad_maximum_fusion), channel_id=1, replica_groups=mesh['fs'=8,'tp'=4] {'tp'}, use_global_device_ids=true, to_apply=%region_5.0 | all-reduce | flops 4 | bytes 32 | tf_op jit(solution)/shard_map/psum | solution.py:92
  236.6 20.0 %psum.43 = f32[4]{0:T(128)S(1)} all-reduce(f32[4]{0:T(128)S(1)} %psum.42), channel_id=1, replica_groups=mesh['fs'=8,'tp'=4] {'fs'}, use_global_device_ids=true, to_apply=%region_6.0 | all-reduce | flops 4 | bytes 32 | tf_op jit(solution)/shard_map/psum | solution.py:92
  256.9 1.9 convolution_convert_fusion
  258.7 1.9 copy.53
  260.6 2.3 convolution_convert_fusion.1
  262.9 1.7 convolution_convert_fusion.2
  266.7 1.0 multiply_bitcast_fusion
  267.9 1.7 subtract_convert_fusion.1
  271.2 2.6 subtract_convert_fusion
  273.8 1.3 copy.48
  275.1 1.8 copy.49
  276.9 1.5 convolution_convert_fusion.3
  278.3 33.0 %psum.47 = bf16[2,64,64]{2,1,0:T(8,128)(2,1)S(1)} all-reduce(bf16[2,64,64]{2,1,0:T(8,128)(2,1)S(1)} %convolution_convert_fusion.3), channel_id=1, replica_groups=mesh['fs'=8,'tp'=4] {'fs'}, use_global_device_ids=true, to_apply=%region_10.0 | all-reduce | flops 8192 | bytes 32768 | tf_op jit(solution)/shard_map/psum | solution.py:84
  312.0 19.5 %all-reduce.4.cloned.1.call-done = bf16[8,64,64]{2,1,0:T(8,128)(2,1)} async-done(((bf16[8,64,64]{2,1,0:T(8,128)(2,1)}), bf16[8,64,64]{2,1,0:T(8,128)(2,1)}) %all-reduce.4.cloned.1.call-update) | async-done | bytes 65552 | tf_op jit(solution)/shard_map/psum | solution.py:83
  331.5 1.8 multiply_add_fusion.3
  333.3 34.4 %all-reduce.6.cloned.1.call-done = (bf16[2,256,256]{2,1,0:T(8,128)(2,1)}, bf16[2,256,256]{2,1,0:T(8,128)(2,1)}) async-done(((bf16[2,256,256]{2,1,0:T(8,128)(2,1)}, bf16[2,256,256]{2,1,0:T(8,128)(2,1)}), (bf16[2,256,256]{2,1,0:T(8,128)(2,1)}, bf16[2,256,256]{2,1,0:T(8,128)(2,1)})) %all-reduce.6.cloned.1.call-update) | async-done | bytes 524304 | tf_op jit(solution)/shard_map/psum | solution.py:87
  367.8 2.2 multiply_add_fusion.1
  369.9 40.3 %all-gather.5.cloned.1.call-done = bf16[4096,128]{1,0:T(8,128)(2,1)} async-done(((bf16[512,128]{1,0:T(8,128)(2,1)}), bf16[4096,128]{1,0:T(8,128)(2,1)}) %all-gather.5.cloned.1.call-update) | async-done | bytes 1048592 | tf_op jit(solution)/shard_map/all_gather | solution.py:111
  410.2 74.1 %all-gather.3.cloned.1.call-done = bf16[4096,512]{1,0:T(8,128)(2,1)} async-done(((bf16[512,512]{1,0:T(8,128)(2,1)}), bf16[4096,512]{1,0:T(8,128)(2,1)}) %all-gather.3.cloned.1.call-update) | async-done | bytes 4194320 | tf_op jit(solution)/shard_map/all_gather | solution.py:110
  484.3 4.6 copy.67
  (41 shorter events, 5.0 us)
Async XLA Ops:
  7.2 215.3 %copy-start = (bf16[2,256,256]{2,1,0:T(8,128)(2,1)S(1)}, bf16[2,256,256]{2,1,0:T(8,128)(2,1)}, u32[]{:S(2)}) copy-start(bf16[2,256,256]{2,1,0:T(8,128)(2,1)} %param.26) | copy-start | bytes 786436
  7.2 202.9 %reduce-scatter.2.cloned.1.call-start = ((), (), s32[]{:S(2)}) async-start(), calls=%async_computation.1 | async-start | bytes 11796480 | tf_op jit(solution)/shard_map/reduce_scatter | solution.py:70
  28.5 1.2 copy-start.4
  28.5 1.6 copy-start.9
  28.6 183.7 %copy-start.10 = (bf16[8,64,64]{2,1,0:T(8,128)(2,1)S(1)}, bf16[8,64,64]{2,1,0:T(8,128)(2,1)}, u32[]{:S(2)}) copy-start(bf16[8,64,64]{2,1,0:T(8,128)(2,1)} %param.28) | copy-start | bytes 196612
  28.6 303.0 %all-reduce.4.cloned.1.call-start = ((), (), s32[]{:S(2)}) async-start(), calls=%async_computation.2 | async-start | bytes 262144 | tf_op jit(solution)/shard_map/psum | solution.py:83
  218.1 0.7 copy-start.3
  258.7 12.3 %copy-start.1 = (f32[2,512,256]{1,2,0:T(8,128)S(1)}, f32[2,512,256]{1,2,0:T(8,128)}, u32[]{:S(2)}) copy-start(f32[2,512,256]{1,2,0:T(8,128)} %get-tuple-element.45) | copy-start | bytes 3145732
  264.7 103.1 %all-reduce.6.cloned.1.call-start = ((), (), s32[]{:S(2)}) async-start(), calls=%async_computation.5 | async-start | bytes 1048576 | tf_op jit(solution)/shard_map/psum | solution.py:87
  266.7 143.5 %all-gather.5.cloned.1.call-start = ((), (), s32[]{:S(2)}) async-start(), calls=%async_computation.4 | async-start | bytes 1179648 | tf_op jit(solution)/shard_map/all_gather | solution.py:111
  267.9 3.2 copy-start.6
  269.6 214.6 %all-gather.3.cloned.1.call-start = ((), (), s32[]{:S(2)}) async-start(), calls=%async_computation.3 | async-start | bytes 4718592 | tf_op jit(solution)/shard_map/all_gather | solution.py:110
  271.0 40.3 %copy-start.11 = (f32[2,64,64]{2,1,0:T(8,128)S(1)}, f32[2,64,64]{2,1,0:T(8,128)}, u32[]{:S(2)}) copy-start(f32[2,64,64]{2,1,0:T(8,128)} %param.25) | copy-start | bytes 98308
  271.1 98.8 %copy-start.2 = (f32[2,512,256]{1,2,0:T(8,128)}, f32[2,512,256]{1,2,0:T(8,128)S(1)}, u32[]{:S(2)}) copy-start(f32[2,512,256]{1,2,0:T(8,128)S(1)} %broadcast_multiply_fusion) | copy-start | bytes 3145732
  271.2 96.6 %copy-start.7 = (f32[2,256,256]{2,1,0:T(8,128)S(1)}, f32[2,256,256]{2,1,0:T(8,128)}, u32[]{:S(2)}) copy-start(f32[2,256,256]{2,1,0:T(8,128)} %param.23) | copy-start | bytes 1572868
  271.2 96.6 %copy-start.8 = (f32[2,256,256]{2,1,0:T(8,128)S(1)}, f32[2,256,256]{2,1,0:T(8,128)}, u32[]{:S(2)}) copy-start(f32[2,256,256]{2,1,0:T(8,128)} %param.22) | copy-start | bytes 1572868
  484.2 4.6 copy-start.5
Sparse Core Ops, SparseCore 0:
  28.7 181.3 reduce-scatter.1
  264.8 66.6 all-reduce.3
  335.1 32.5 all-reduce.5
  369.7 40.3 all-gather.4
  412.7 71.4 all-gather.2
